TPU v7x, 512 devices: a whole 4x4x16 slice. The times are simulated.
512 devices in a mesh: ep: 32 (over z, core), tp: 16 (over y, x).
Axes of the slice: x: 4, y: 4, z: 16, core: 2. Of those that a mesh axis runs over, the one named last changes fastest.
Arguments:
- tokens: bfloat16 [8192, 2048], P('ep', 'tp'), may hold values from -800 to 800
- norm_gain: bfloat16 [2048], P('tp'), may hold values from 0.099609375 to 1.8984375
- w_gate: bfloat16 [32, 2048, 6144], P('ep', None, 'tp'), may hold values from -0.125 to 0.125
- w_up: bfloat16 [32, 2048, 6144], P('ep', None, 'tp'), may hold values from -0.125 to 0.125
- w_down: bfloat16 [32, 6144, 2048], P('ep', 'tp'), may hold values from -1.2757759 to 1.2757759
- routes: int32 [8192, 2], P('ep'), may hold values from 0 to 31, all different within a row; in each aligned block of 256 rows (0 to 255, 256 to 511, ...) at most 32 rows name the same one
- route_weights: float32 [8192, 2], P('ep'), may hold values from 0.1 to 1
- final_gain: bfloat16 [2048], P('tp'), may hold values from 0.099609375 to 1.8984375
Outputs:
- mixed_out: bfloat16 [8192, 2048], P('ep', 'tp')
Inputs may be any that keep to these rules, and one draw needn't show every extreme that they name: `routes`: A token's 2 experts differ. Among the tokens of one index of ep (aligned blocks of 256 rows), no expert is named by more than 32 tokens, a bound that some block reaches.
All inputs are finite; a program needn't handle non-finite values.
Results may differ from a plain program's by a relative error of at most 0.017.
Values may be sent and summed in bfloat16 or wider, within the bound.
A program may use at most 64 MiB of HBM per device.

v0:
```python
import jax
import jax.numpy as jnp
from jax import lax
from jax.sharding import PartitionSpec as P

EPS = 1e-06


def from_everyone(shard, axis):
    copies = jnp.broadcast_to(shard, (lax.axis_size(axis), *shard.shape))
    return lax.all_to_all(copies, axis, split_axis=0, concat_axis=0, tiled=True)


def over_copies(shard, axis):
    return from_everyone(shard, axis).sum(axis=0)


def cut_along(shard, dim, length):
    before, after = (shard.shape[:dim], shard.shape[dim + 1 :])
    return jnp.moveaxis(shard.reshape(*before, length, -1, *after), dim, 0)


def summed_on_arrival(shard, axis, dim):
    length = lax.axis_size(axis)
    tiles = lax.all_to_all(cut_along(shard, dim, length), axis, 0, 0, tiled=True)
    return jnp.sum(tiles.astype(jnp.float32), axis=0)


def slot_targets(routes, experts, capacity):
    flat = routes.reshape(-1)
    onehot = (flat[:, None] == jnp.arange(experts, dtype=jnp.int32)[None, :]).astype(jnp.int32)
    before = jnp.cumsum(onehot, axis=0) - onehot
    slot = jnp.sum(before * onehot, axis=1)
    return flat * capacity + slot


def local(tokens, norm_gain, w_gate, w_up, w_down, routes, route_weights, final_gain):
    experts = lax.axis_size("ep")
    tok_rows = tokens.shape[0]
    share = tokens.shape[1]
    width = share * lax.axis_size("tp")
    topk = routes.shape[1]
    capacity = 2 * tok_rows * topk // experts
    wide = tokens.astype(jnp.float32)
    input_squares = over_copies(jnp.sum(wide * wide, axis=1), "tp")
    scale = lax.rsqrt(input_squares / width + EPS)
    normed = (wide * scale[:, None] * norm_gain.astype(jnp.float32)[None, :]).astype(jnp.bfloat16)
    target = slot_targets(routes, experts, capacity)
    sources = jnp.repeat(jnp.arange(tok_rows, dtype=jnp.int32), topk)
    gate_w = w_gate[0]
    up_w = w_up[0]
    down_w = w_down[0]
    outbox = jnp.zeros((experts * capacity, share), jnp.bfloat16).at[target].set(normed[sources])
    inbox = lax.all_to_all(outbox, "ep", split_axis=0, concat_axis=0, tiled=True)
    piece = lax.all_gather(inbox, "tp", axis=1, tiled=True)
    gate = jnp.dot(piece, gate_w, preferred_element_type=jnp.float32)
    up = jnp.dot(piece, up_w, preferred_element_type=jnp.float32)
    hidden = (jax.nn.silu(gate) * up).astype(jnp.bfloat16)
    sums = summed_on_arrival(
        lax.dot_general(
            down_w, hidden, (((0,), (1,)), ((), ())), preferred_element_type=jnp.float32
        ).astype(jnp.bfloat16),
        "tp",
        0,
    )
    returned = lax.all_to_all(
        sums.astype(jnp.bfloat16), "ep", split_axis=1, concat_axis=1, tiled=True
    )
    picked = jnp.take(returned, target, axis=1).reshape(returned.shape[0], tok_rows, topk)
    combined = jnp.einsum("dtk,tk->td", picked.astype(jnp.float32), route_weights)
    local_squares = jnp.sum(combined * combined, axis=1)
    total_squares = over_copies(local_squares, "tp")
    final_scale = lax.rsqrt(total_squares / width + EPS)
    return (combined * final_scale[:, None] * final_gain.astype(jnp.float32)[None, :]).astype(
        jnp.bfloat16
    )


def solution(mesh):
    in_specs = (
        P("ep", "tp"),
        P("tp"),
        P("ep", None, "tp"),
        P("ep", None, "tp"),
        P("ep", "tp", None),
        P("ep", None),
        P("ep", None),
        P("tp"),
    )
    out_specs = P("ep", "tp")
    return jax.shard_map(local, mesh=mesh, in_specs=in_specs, out_specs=out_specs, check_vma=False)
```

profile of v0, /device:TPU:1, one launch (start us, length us, event | category | flops | bytes accessed | tf_op | source)
XLA Modules:
  0.0 259.8 jit_solution(18186526171175588482)
XLA Ops:
  6.5 0.0 copy-start
  6.5 0.0 copy-start.3
  6.5 1.1 fusion.9
  7.6 0.6 broadcast_in_dim.31
  8.3 7.6 %all-to-all-start = ((f32[16,1,256]{2,1,0:T(1,128)}), f32[16,1,256]{2,1,0:T(1,128)S(1)}, u32[]{:S(2)}, u32[]{:S(2)}) async-start(f32[16,1,256]{2,1,0:T(1,128)} %broadcast_in_dim.31), calls=%async_computation | async-start | bytes 32768 | tf_op jit(solution)/shard_map/all_to_all | solution.py:11
  15.8 0.0 all-gather.2.cloned.1.call-start
  15.9 0.8 copy.31
  16.7 0.1 eq.26
  16.9 0.1 reshape.120
  17.0 0.7 broadcast_multiply_fusion
  17.7 1.2 reduce-window.6
  18.9 0.2 slice_reduce_fusion
  19.1 0.1 copy.36
  19.3 0.1 mul.70
  19.4 0.1 reshape.122
  19.6 0.1 fusion.18
  19.7 0.7 convert_element_type.37
  20.4 1.9 all-to-all-done
  22.3 0.9 fusion.11
  23.3 3.1 %scatter_custom_fusion = bf16[1024,128]{1,0:T(8,128)(2,1)S(1)} fusion(s32[512]{0:T(512)S(1)} %bitcast.62, bf16[256,128]{1,0:T(8,128)(2,1)S(1)} %fusion.11, s32[1024]{0:T(1024)S(1)} %pad_clamp_fusion.1, bf16[]{:T(256)} %constant.34.clone.1), kind=kCustom, calls=%fused_computation.17 | custom fusion | bytes 262146 | tf_op jit(solution)/shard_map/scatter | solution.py:53
  26.3 39.5 %all_to_all.41 = bf16[32,32,128]{2,1,0:T(8,128)(2,1)} all-to-all(bf16[32,32,128]{2,1,0:T(8,128)(2,1)S(1)} %bitcast.57), channel_id=1, replica_groups=mesh['ep'=32,'tp'=16] {'ep'}, dimensions={0} | all-to-all | bytes 524288 | tf_op jit(solution)/shard_map/all_to_all | solution.py:54
  65.9 0.0 all-gather.2.cloned.1.call-update
  65.9 59.4 %all-gather.2.cloned.1.call-done = bf16[1024,2048]{1,0:T(8,128)(2,1)} async-done(((bf16[1024,128]{1,0:T(8,128)(2,1)}), bf16[1024,2048]{1,0:T(8,128)(2,1)}) %all-gather.2.cloned.1.call-update) | async-done | bytes 4194320 | tf_op jit(solution)/shard_map/all_gather | solution.py:55
  125.3 0.0 copy-done.3
  125.3 5.7 %fusion.3 = f32[1024,384]{1,0:T(8,128)} fusion(bf16[1024,2048]{1,0:T(8,128)(2,1)} %all-gather.2.cloned.1.call-done, bf16[1,2048,384]{2,1,0:T(8,128)(2,1)S(1)} %copy-done.3), kind=kOutput, calls=%fused_computation.8 | convolution fusion | flops 1610612736 | bytes 7340032 | tf_op jit(solution)/shard_map/dot_general | solution.py:56
  131.0 0.0 copy-done
  131.0 9.6 %convert_bitcast_fusion = bf16[128,16,8,128]{3,2,1,0:T(8,128)(2,1)} fusion(bf16[1,384,2048]{2,1,0:T(8,128)(2,1)S(1)} %copy-done, f32[1024,384]{1,0:T(8,128)} %fusion.3, bf16[1024,2048]{1,0:T(8,128)(2,1)} %all-gather.2.cloned.1.call-done, bf16[1,2048,384]{2,1,0:T(8,128)(2,1)} %param.11), kind=kOutput, calls=%fused_computation.4 | convolution fusion | flops 3225681920 | bytes 13107200 | tf_op jit(solution)/shard_map/dot_general | solution.py:60
  140.6 3.3 %copy.48 = bf16[128,16,8,128]{3,2,0,1:T(8,128)(2,1)S(1)} copy(bf16[128,16,8,128]{3,2,1,0:T(8,128)(2,1)} %convert_bitcast_fusion) | data formatting | bytes 8388608 | tf_op jit(solution)/shard_map/reshape | solution.py:20
  143.9 54.5 %all_to_all.42 = bf16[16,128,1024]{1,2,0:T(8,128)(2,1)} all-to-all(bf16[16,128,1024]{1,2,0:T(8,128)(2,1)S(1)} %bitcast.54), channel_id=1, replica_groups=mesh['ep'=32,'tp'=16] {'tp'}, dimensions={0} | all-to-all | bytes 8388608 | tf_op jit(solution)/shard_map/all_to_all | solution.py:25
  198.3 0.0 copy-start.1
  198.3 0.0 copy-start.2
  198.3 3.5 %reduce_sum.66 = bf16[128,1024]{0,1:T(8,128)(2,1)} reduce(bf16[16,128,1024]{1,2,0:T(8,128)(2,1)} %all_to_all.42, bf16[]{:T(256)} %constant.34.clone.1), dimensions={0}, to_apply=%region_6.7 | reduce | flops 1966080 | bytes 4456450 | tf_op jit(solution)/shard_map/reduce_sum | solution.py:26
  201.9 15.5 %all-to-all-start.3 = ((bf16[128,32,32]{0,2,1:T(8,128)(2,1)}), bf16[128,32,32]{0,2,1:T(8,128)(2,1)S(1)}, u32[]{:S(2)}, u32[]{:S(2)}) async-start(bf16[128,32,32]{0,2,1:T(8,128)(2,1)} %bitcast.10), calls=%async_computation.3 | async-start | bytes 524288 | tf_op jit(solution)/shard_map/all_to_all | solution.py:66
  217.4 0.1 reduce_sum.62
  217.5 0.1 copy.34
  217.6 0.0 copy-done.1
  217.6 0.2 copy.35
  217.8 0.0 copy-done.2
  217.8 0.2 copy.40
  218.0 21.6 %all-to-all-done.3 = bf16[128,32,32]{0,2,1:T(8,128)(2,1)S(1)} async-done(((bf16[128,32,32]{0,2,1:T(8,128)(2,1)}), bf16[128,32,32]{0,2,1:T(8,128)(2,1)S(1)}, u32[]{:S(2)}, u32[]{:S(2)}) %all-to-all-start.3) | async-done | bytes 262176 | tf_op jit(solution)/shard_map/all_to_all | solution.py:66
  239.7 0.0 copy-start.4
  239.7 1.3 gather_fusion
  241.0 0.5 fusion.15
  241.5 0.1 multiply_reduce_fusion
  241.6 0.6 broadcast_in_dim.34
  242.2 3.5 %all-to-all-start.4 = ((f32[16,1,256]{2,1,0:T(1,128)}), f32[16,1,256]{2,1,0:T(1,128)S(1)}, u32[]{:S(2)}, u32[]{:S(2)}) async-start(f32[16,1,256]{2,1,0:T(1,128)} %broadcast_in_dim.34), calls=%async_computation.4 | async-start | bytes 32768 | tf_op jit(solution)/shard_map/all_to_all | solution.py:11
  245.8 0.0 copy-done.4
  245.8 6.4 %all-to-all-done.4 = f32[16,1,256]{2,1,0:T(1,128)S(1)} async-done(((f32[16,1,256]{2,1,0:T(1,128)}), f32[16,1,256]{2,1,0:T(1,128)S(1)}, u32[]{:S(2)}, u32[]{:S(2)}) %all-to-all-start.4) | async-done | bytes 16416 | tf_op jit(solution)/shard_map/all_to_all | solution.py:11
  252.2 0.7 multiply_convert_fusion.1
  (14 shorter events, 0.2 us)
Async XLA Ops:
  6.5 124.5 %copy-start = (bf16[1,384,2048]{2,1,0:T(8,128)(2,1)S(1)}, bf16[1,384,2048]{2,1,0:T(8,128)(2,1)}, u32[]{:S(2)}) copy-start(bf16[1,384,2048]{2,1,0:T(8,128)(2,1)} %param.12) | copy-start | bytes 4718596
  6.5 118.7 %copy-start.3 = (bf16[1,2048,384]{2,1,0:T(8,128)(2,1)S(1)}, bf16[1,2048,384]{2,1,0:T(8,128)(2,1)}, u32[]{:S(2)}) copy-start(bf16[1,2048,384]{2,1,0:T(8,128)(2,1)} %param.10) | copy-start | bytes 4718596
  8.3 14.0 %all-to-all-start = ((f32[16,1,256]{2,1,0:T(1,128)}), f32[16,1,256]{2,1,0:T(1,128)S(1)}, u32[]{:S(2)}, u32[]{:S(2)}) async-start(f32[16,1,256]{2,1,0:T(1,128)} %broadcast_in_dim.31), calls=%async_computation | async-start | bytes 32768 | tf_op jit(solution)/shard_map/all_to_all | solution.py:11
  15.8 109.4 %all-gather.2.cloned.1.call-start = ((), (), s32[]{:S(2)}) async-start(), calls=%async_computation.5 | async-start | bytes 4456448 | tf_op jit(solution)/shard_map/all_gather | solution.py:55
  198.3 19.3 %copy-start.1 = (s32[256,2]{0,1:T(2,128)S(1)}, s32[256,2]{0,1:T(2,128)}, u32[]{:S(2)}) copy-start(s32[256,2]{0,1:T(2,128)} %param.13) | copy-start | bytes 6148
  198.3 19.5 %copy-start.2 = (f32[256,2]{0,1:T(2,128)S(1)}, f32[256,2]{0,1:T(2,128)}, u32[]{:S(2)}) copy-start(f32[256,2]{0,1:T(2,128)} %param.14) | copy-start | bytes 6148
  201.9 37.8 %all-to-all-start.3 = ((bf16[128,32,32]{0,2,1:T(8,128)(2,1)}), bf16[128,32,32]{0,2,1:T(8,128)(2,1)S(1)}, u32[]{:S(2)}, u32[]{:S(2)}) async-start(bf16[128,32,32]{0,2,1:T(8,128)(2,1)} %bitcast.10), calls=%async_computation.3 | async-start | bytes 524288 | tf_op jit(solution)/shard_map/all_to_all | solution.py:66
  239.7 6.1 %copy-start.4 = (bf16[128]{0:T(256)(128)(2,1)S(1)}, bf16[128]{0:T(256)(128)(2,1)}, u32[]{:S(2)}) copy-start(bf16[128]{0:T(256)(128)(2,1)} %param.15) | copy-start | bytes 772
  242.2 9.9 %all-to-all-start.4 = ((f32[16,1,256]{2,1,0:T(1,128)}), f32[16,1,256]{2,1,0:T(1,128)S(1)}, u32[]{:S(2)}, u32[]{:S(2)}) async-start(f32[16,1,256]{2,1,0:T(1,128)} %broadcast_in_dim.34), calls=%async_computation.4 | async-start | bytes 32768 | tf_op jit(solution)/shard_map/all_to_all | solution.py:11
Sparse Core Ops, SparseCore 0:
  66.0 59.2 all-gather.1
where the time goes:
time: 260 us
  blocking collectives  94 us (36%)
  waiting for transfers between devices  89.3 us (34%)
  starting transfers between devices  26.6 us (10%)
  matrix products  15.8 us (6%)
  between operations  13.6 us (5%)
  local copies, waits for them, and re-layouts  11.2 us (4%)
  other arithmetic  9.22 us (4%)
    all_gather x1, waiting for transfers between devices, local(): piece = lax.all_gather(inbox, 'tp', axis=1, tiled=True)  59.4 us
    all_to_all x1, blocking collectives, summed_on_arrival(): lax.all_to_all(cut_along(shard, dim, length), axis, 0, 0, tiled=True)  54.5 us
    all_to_all x1, blocking collectives, local(): lax.all_to_all(outbox, 'ep', split_axis=0, concat_axis=0, tiled=True)  39.5 us
    all_to_all x1, waiting for transfers between devices, local(): lax.all_to_all(sums.astype(jnp.bfloat16), 'ep', split_axis=1, concat_axis...  21.6 us
    all_to_all x1, starting transfers between devices, local(): lax.all_to_all(sums.astype(jnp.bfloat16), 'ep', split_axis=1, concat_axis...  15.5 us
    all_to_all x2, starting transfers between devices, from_everyone(): return lax.all_to_all(copies, axis, split_axis=0, concat_axis=0, tiled=True)  11.1 us
    dot_general x1, matrix products, local(): lax.dot_general(down_w, hidden, (((0,), (1,)), ((), ())), preferred_eleme...  9.6 us
    all_to_all x2, waiting for transfers between devices, from_everyone(): return lax.all_to_all(copies, axis, split_axis=0, concat_axis=0, tiled=True)  8.25 us
  transfers between devices with their start and end apart: 4, of which 4 were waited for; matrix products, arithmetic and copies ran while one was open for 2% of the time, Pallas kernels for 0%

commit v1 on v0

--- a/solution.py
+++ b/solution.py
@@ -52,7 +52,8 @@
     down_w = w_down[0]
     outbox = jnp.zeros((experts * capacity, share), jnp.bfloat16).at[target].set(normed[sources])
     inbox = lax.all_to_all(outbox, "ep", split_axis=0, concat_axis=0, tiled=True)
-    piece = lax.all_gather(inbox, "tp", axis=1, tiled=True)
+    copies_2 = jnp.concatenate([inbox] * lax.axis_size("tp"), axis=1)
+    piece = lax.all_to_all(copies_2, "tp", 1, 1, tiled=True)
     gate = jnp.dot(piece, gate_w, preferred_element_type=jnp.float32)
     up = jnp.dot(piece, up_w, preferred_element_type=jnp.float32)
     hidden = (jax.nn.silu(gate) * up).astype(jnp.bfloat16)

time: 260 us -> 239 us (0.919)
  waiting for transfers between devices: 89.3 us -> 29.9 us
  blocking collectives: 94 us -> 146 us
  between operations: 13.6 us -> 0.21 us
  starting transfers between devices: 26.6 us -> 18.4 us
  local copies, waits for them, and re-layouts: 11.2 us -> 18.4 us
    all_gather x1 -> x0, waiting for transfers between devices: 59.4 us -> none  [local(): piece = lax.all_gather(inbox, 'tp', axis=1, tiled=True)]
    all_to_all x0 -> x1, blocking collectives: none -> 53.5 us  [local(): piece = lax.all_to_all(copies_2, 'tp', 1, 1, tiled=True)]
    all_to_all x1, starting transfers between devices: 15.5 us -> 7.29 us  [local(): lax.all_to_all(sums.astype(jnp.bfloat16), 'ep', split_axis=1, concat_axis...]
    all_to_all x0 -> x1, local copies, waits for them, and re-layouts: none -> 6.4 us  [local(): piece = lax.all_to_all(copies_2, 'tp', 1, 1, tiled=True)]
  transfers between devices with their start and end apart: 4 -> 3, of which waited for: 4 -> 3; matrix products, arithmetic and copies ran while one was open for 2% -> 2% of each run, Pallas kernels for 0% -> 0%
where the time goes in v1:
time: 239 us
  blocking collectives  146 us (61%)
  waiting for transfers between devices  29.9 us (13%)
  local copies, waits for them, and re-layouts  18.4 us (8%)
  starting transfers between devices  18.4 us (8%)
  matrix products  16.4 us (7%)
  other arithmetic  9.19 us (4%)
    all_to_all x1, blocking collectives, local(): piece = lax.all_to_all(copies_2, 'tp', 1, 1, tiled=True)  53.5 us
    all_to_all x1, blocking collectives, summed_on_arrival(): lax.all_to_all(cut_along(shard, dim, length), axis, 0, 0, tiled=True)  53.1 us
    all_to_all x1, blocking collectives, local(): lax.all_to_all(outbox, 'ep', split_axis=0, concat_axis=0, tiled=True)  39.4 us
    all_to_all x1, waiting for transfers between devices, local(): lax.all_to_all(sums.astype(jnp.bfloat16), 'ep', split_axis=1, concat_axis...  21.6 us
    all_to_all x2, starting transfers between devices, from_everyone(): return lax.all_to_all(copies, axis, split_axis=0, concat_axis=0, tiled=True)  11.1 us
    dot_general x1, matrix products, local(): lax.dot_general(down_w, hidden, (((0,), (1,)), ((), ())), preferred_eleme...  9.64 us
    all_to_all x2, waiting for transfers between devices, from_everyone(): return lax.all_to_all(copies, axis, split_axis=0, concat_axis=0, tiled=True)  8.3 us
    all_to_all x1, starting transfers between devices, local(): lax.all_to_all(sums.astype(jnp.bfloat16), 'ep', split_axis=1, concat_axis...  7.29 us
  transfers between devices with their start and end apart: 3, of which 3 were waited for; matrix products, arithmetic and copies ran while one was open for 2% of the time, Pallas kernels for 0%

profile of v1, /device:TPU:1, one launch (start us, length us, event | category | flops | bytes accessed | tf_op | source)
XLA Modules:
  0.0 238.5 jit_solution(1083678155574832405)
XLA Ops:
  0.0 0.0 copy-start
  0.0 1.1 fusion.9
  1.1 0.6 broadcast_in_dim.31
  1.7 7.6 %all-to-all-start = ((f32[16,1,256]{2,1,0:T(1,128)}), f32[16,1,256]{2,1,0:T(1,128)S(1)}, u32[]{:S(2)}, u32[]{:S(2)}) async-start(f32[16,1,256]{2,1,0:T(1,128)} %broadcast_in_dim.31), calls=%async_computation | async-start | bytes 32768 | tf_op jit(solution)/shard_map/all_to_all | solution.py:11
  9.3 0.8 copy.39
  10.1 0.1 eq.26
  10.2 0.1 reshape.156
  10.4 0.7 broadcast_multiply_fusion
  11.1 1.2 reduce-window.6
  12.3 0.2 slice_reduce_fusion
  12.5 0.1 copy.44
  12.7 0.1 mul.70
  12.8 0.1 reshape.158
  13.0 0.1 fusion.18
  13.1 0.7 convert_element_type.37
  13.8 1.9 all-to-all-done
  15.8 0.9 fusion.11
  16.7 3.1 %scatter_custom_fusion = bf16[1024,128]{1,0:T(8,128)(2,1)S(1)} fusion(s32[512]{0:T(512)S(1)} %bitcast.65, bf16[256,128]{1,0:T(8,128)(2,1)S(1)} %fusion.11, s32[1024]{0:T(1024)S(1)} %pad_clamp_fusion.1, bf16[]{:T(256)} %constant.34.clone.1), kind=kCustom, calls=%fused_computation.17 | custom fusion | bytes 262146 | tf_op jit(solution)/shard_map/scatter | solution.py:53
  19.8 39.4 %all_to_all.47 = bf16[32,32,128]{2,1,0:T(8,128)(2,1)S(1)} all-to-all(bf16[32,32,128]{2,1,0:T(8,128)(2,1)S(1)} %bitcast.60), channel_id=1, replica_groups=mesh['ep'=32,'tp'=16] {'ep'}, dimensions={0} | all-to-all | bytes 524288 | tf_op jit(solution)/shard_map/all_to_all | solution.py:54
  59.2 0.8 concatenate.7
  60.0 53.5 %all_to_all.48 = bf16[1024,16,128]{2,0,1:T(8,128)(2,1)} all-to-all(bf16[1024,16,128]{2,0,1:T(8,128)(2,1)S(1)} %concatenate.7), channel_id=1, replica_groups=mesh['ep'=32,'tp'=16] {'tp'}, dimensions={1} | all-to-all | bytes 8388608 | tf_op jit(solution)/shard_map/all_to_all | solution.py:56
  113.5 6.4 %copy.46 = bf16[1024,16,128]{0,2,1:T(8,128)(2,1)} copy(bf16[1024,16,128]{2,0,1:T(8,128)(2,1)} %all_to_all.48) | data formatting | bytes 8388608 | tf_op jit(solution)/shard_map/all_to_all | solution.py:56
  119.9 6.3 %fusion.3 = f32[1024,384]{1,0:T(8,128)} fusion(bf16[1024,2048]{0,1:T(8,128)(2,1)} %bitcast.57, bf16[1,2048,384]{2,1,0:T(8,128)(2,1)} %param.10), kind=kOutput, calls=%fused_computation.8 | convolution fusion | flops 1610612736 | bytes 7340032 | tf_op jit(solution)/shard_map/dot_general | solution.py:57
  126.2 0.0 copy-done
  126.2 9.6 %convert_bitcast_fusion = bf16[128,16,8,128]{3,2,1,0:T(8,128)(2,1)} fusion(bf16[1,384,2048]{2,1,0:T(8,128)(2,1)S(1)} %copy-done, f32[1024,384]{1,0:T(8,128)} %fusion.3, bf16[1024,2048]{0,1:T(8,128)(2,1)} %bitcast.58, bf16[1,2048,384]{2,1,0:T(8,128)(2,1)} %param.11), kind=kOutput, calls=%fused_computation.4 | convolution fusion | flops 3225681920 | bytes 13107200 | tf_op jit(solution)/shard_map/dot_general | solution.py:61
  135.8 3.3 %copy.57 = bf16[128,16,8,128]{3,2,0,1:T(8,128)(2,1)S(1)} copy(bf16[128,16,8,128]{3,2,1,0:T(8,128)(2,1)} %convert_bitcast_fusion) | data formatting | bytes 8388608 | tf_op jit(solution)/shard_map/reshape | solution.py:20
  139.1 53.1 %all_to_all.49 = bf16[16,128,1024]{1,2,0:T(8,128)(2,1)} all-to-all(bf16[16,128,1024]{1,2,0:T(8,128)(2,1)S(1)} %bitcast.55), channel_id=1, replica_groups=mesh['ep'=32,'tp'=16] {'tp'}, dimensions={0} | all-to-all | bytes 8388608 | tf_op jit(solution)/shard_map/all_to_all | solution.py:25
  192.2 0.0 copy-start.1
  192.2 0.0 copy-start.2
  192.2 3.5 %reduce_sum.66 = bf16[128,1024]{0,1:T(8,128)(2,1)} reduce(bf16[16,128,1024]{1,2,0:T(8,128)(2,1)} %all_to_all.49, bf16[]{:T(256)} %constant.34.clone.1), dimensions={0}, to_apply=%region_6.7 | reduce | flops 1966080 | bytes 4456450 | tf_op jit(solution)/shard_map/reduce_sum | solution.py:26
  195.7 7.3 %all-to-all-start.4 = ((bf16[128,32,32]{0,2,1:T(8,128)(2,1)}), bf16[128,32,32]{0,2,1:T(8,128)(2,1)S(1)}, u32[]{:S(2)}, u32[]{:S(2)}) async-start(bf16[128,32,32]{0,2,1:T(8,128)(2,1)} %bitcast.11), calls=%async_computation.4 | async-start | bytes 524288 | tf_op jit(solution)/shard_map/all_to_all | solution.py:67
  203.0 0.1 reduce_sum.62
  203.2 0.1 copy.42
  203.2 0.0 copy-done.1
  203.3 0.2 copy.43
  203.4 0.0 copy-done.2
  203.4 0.2 copy.49
  203.6 21.6 %all-to-all-done.4 = bf16[128,32,32]{0,2,1:T(8,128)(2,1)S(1)} async-done(((bf16[128,32,32]{0,2,1:T(8,128)(2,1)}), bf16[128,32,32]{0,2,1:T(8,128)(2,1)S(1)}, u32[]{:S(2)}, u32[]{:S(2)}) %all-to-all-start.4) | async-done | bytes 262176 | tf_op jit(solution)/shard_map/all_to_all | solution.py:67
  225.3 0.0 copy-start.3
  225.3 1.3 gather_fusion
  226.6 0.5 fusion.15
  227.1 0.1 multiply_reduce_fusion
  227.2 0.6 broadcast_in_dim.34
  227.9 3.5 %all-to-all-start.5 = ((f32[16,1,256]{2,1,0:T(1,128)}), f32[16,1,256]{2,1,0:T(1,128)S(1)}, u32[]{:S(2)}, u32[]{:S(2)}) async-start(f32[16,1,256]{2,1,0:T(1,128)} %broadcast_in_dim.34), calls=%async_computation.5 | async-start | bytes 32768 | tf_op jit(solution)/shard_map/all_to_all | solution.py:11
  231.4 0.0 copy-done.3
  231.4 6.4 %all-to-all-done.5 = f32[16,1,256]{2,1,0:T(1,128)S(1)} async-done(((f32[16,1,256]{2,1,0:T(1,128)}), f32[16,1,256]{2,1,0:T(1,128)S(1)}, u32[]{:S(2)}, u32[]{:S(2)}) %all-to-all-start.5) | async-done | bytes 16416 | tf_op jit(solution)/shard_map/all_to_all | solution.py:11
  237.8 0.7 multiply_convert_fusion.1
  (14 shorter events, 0.2 us)
Async XLA Ops:
  0.0 126.2 %copy-start = (bf16[1,384,2048]{2,1,0:T(8,128)(2,1)S(1)}, bf16[1,384,2048]{2,1,0:T(8,128)(2,1)}, u32[]{:S(2)}) copy-start(bf16[1,384,2048]{2,1,0:T(8,128)(2,1)} %param.12) | copy-start | bytes 4718596
  1.7 14.0 %all-to-all-start = ((f32[16,1,256]{2,1,0:T(1,128)}), f32[16,1,256]{2,1,0:T(1,128)S(1)}, u32[]{:S(2)}, u32[]{:S(2)}) async-start(f32[16,1,256]{2,1,0:T(1,128)} %broadcast_in_dim.31), calls=%async_computation | async-start | bytes 32768 | tf_op jit(solution)/shard_map/all_to_all | solution.py:11
  192.2 11.0 %copy-start.1 = (s32[256,2]{0,1:T(2,128)S(1)}, s32[256,2]{0,1:T(2,128)}, u32[]{:S(2)}) copy-start(s32[256,2]{0,1:T(2,128)} %param.13) | copy-start | bytes 6148
  192.2 11.3 %copy-start.2 = (f32[256,2]{0,1:T(2,128)S(1)}, f32[256,2]{0,1:T(2,128)}, u32[]{:S(2)}) copy-start(f32[256,2]{0,1:T(2,128)} %param.14) | copy-start | bytes 6148
  195.7 29.6 %all-to-all-start.4 = ((bf16[128,32,32]{0,2,1:T(8,128)(2,1)}), bf16[128,32,32]{0,2,1:T(8,128)(2,1)S(1)}, u32[]{:S(2)}, u32[]{:S(2)}) async-start(bf16[128,32,32]{0,2,1:T(8,128)(2,1)} %bitcast.11), calls=%async_computation.4 | async-start | bytes 524288 | tf_op jit(solution)/shard_map/all_to_all | solution.py:67
  225.3 6.1 %copy-start.3 = (bf16[128]{0:T(256)(128)(2,1)S(1)}, bf16[128]{0:T(256)(128)(2,1)}, u32[]{:S(2)}) copy-start(bf16[128]{0:T(256)(128)(2,1)} %param.15) | copy-start | bytes 772
  227.9 9.9 %all-to-all-start.5 = ((f32[16,1,256]{2,1,0:T(1,128)}), f32[16,1,256]{2,1,0:T(1,128)S(1)}, u32[]{:S(2)}, u32[]{:S(2)}) async-start(f32[16,1,256]{2,1,0:T(1,128)} %broadcast_in_dim.34), calls=%async_computation.5 | async-start | bytes 32768 | tf_op jit(solution)/shard_map/all_to_all | solution.py:11
